TPU v7x, 32 devices: a whole 2x2x4 slice. The times are simulated.
32 devices in a mesh: sp: 8 (over z, y), tp: 4 (over x, core).
Axes of the slice: x: 2, y: 2, z: 4, core: 2. Of those that a mesh axis runs over, the one named last changes fastest.
Arguments:
- residual: bfloat16 [1536, 2048], P(('sp', 'tp')), may hold values from -6 to 6
- mixer_input: bfloat16 [1536, 512], P('sp', 'tp'), may hold values from -6 to 6
- log_gate: float32 [1536, 32], P('sp', 'tp'), may hold values from -2 to 0
- decay_rate: float32 [2, 32, 64], P(None, 'tp'), may hold values from 0 to 1
- turn_rate: float32 [2, 32, 64], P(None, 'tp'), may hold values from -1 to 1
- drive_real: float32 [2, 32, 16, 64], P(None, 'tp'), may hold values from -1 to 1
- drive_imaginary: float32 [2, 32, 16, 64], P(None, 'tp'), may hold values from -1 to 1
- read_real: float32 [2, 32, 16, 64], P(None, 'tp'), may hold values from -0.75 to 0.75
- read_imaginary: float32 [2, 32, 16, 64], P(None, 'tp'), may hold values from -0.75 to 0.75
- skip_gain: float32 [512], P('tp'), may hold values from -4 to 4
- project_weight: bfloat16 [512, 2048], replicated, may hold values from -0.25 to 0.25
- norm_gain: float32 [2048], replicated, may hold values from 0.1 to 1.9
- final_gain: float32 [2048], replicated, may hold values from 0.1 to 1.9
- routes: int32 [1536, 2], P('sp'), may hold values from 0 to 7, all different within a row; in each aligned block of 48 rows (0 to 47, 48 to 95, ...) at most 18 rows name the same one
- group_weight: float32 [1536], P('sp'), may hold values from 0.2 to 1
- expert_weight: float32 [1536, 2], P('sp'), may hold values from 0.1 to 1
- gate_weight: bfloat16 [8, 2048, 1024], P('sp', None, 'tp'), may hold values from -0.125 to 0.125
- linear_weight: bfloat16 [8, 2048, 1024], P('sp', None, 'tp'), may hold values from -0.125 to 0.125
- down_weight: bfloat16 [8, 1024, 2048], P('sp', 'tp'), may hold values from -0.1875 to 0.1875
Outputs:
- finished: bfloat16 [1536, 2048], P(('sp', 'tp'))
Inputs may be any that keep to these rules, and one draw needn't show every extreme that they name: `routes`: each row names 2 different experts. In each aligned block of 48 rows no expert is named by more than 18 rows; some expert is named by exactly 18 rows of some block.
All inputs are finite; a program needn't handle non-finite values.
Results may differ from a plain program's by a relative error of at most 0.006.
Values may be sent and summed in bfloat16 or wider, within the bound.
A program may use at most 128 MiB of HBM per device.

v0:
```python
import functools

import jax
import jax.numpy as jnp
from jax import lax
from jax.experimental import pallas as pl
from jax.experimental.pallas import tpu as pltpu
from jax.sharding import PartitionSpec as P

deep_alpha = 2.0**0.25
norm_epsilon = 1e-05
highest = lax.Precision.HIGHEST
f32 = jnp.float32
bf16 = jnp.bfloat16
segments = 8


def layer_norm(values, gain):
    center = values - jnp.mean(values, axis=-1, keepdims=True)
    spread = jnp.mean(center * center, axis=-1, keepdims=True)
    return center * lax.rsqrt(spread + norm_epsilon) * gain


def iota(shape, axis):
    return lax.broadcasted_iota(jnp.int32, shape, axis)


def exact_dot(a, b, dims=((1,), (0,))):
    return lax.dot_general(a, b, (dims, ((), ())), precision=highest, preferred_element_type=f32)


def mixer_kernel(n_sp, n_tp, *refs):
    sources, middle_ref, staged = refs[:12], refs[12], refs[13:25]
    (push, gate, seg, enter, total, totals, act, chan) = refs[25:33]
    (stage_sems, send_a, recv_a, send_b, recv_b) = refs[33:]
    loads = [
        pltpu.make_async_copy(source, place, stage_sems.at[i])
        for i, (source, place) in enumerate(zip(sources, staged))
    ]
    for load in loads:
        load.start()
    (x_ref, gate_ref, decay_ref, turn_ref, drive_re, drive_im) = staged[:6]
    (read_re, read_im, skip_ref, residual_ref, gain_ref, weight) = staged[6:]
    sp = lax.axis_index("sp")
    tp = lax.axis_index("tp")
    barrier = pltpu.get_barrier_semaphore()
    for k in range(1, n_sp):
        pl.semaphore_signal(barrier, inc=1, device_id={"sp": lax.rem(sp + k, n_sp)})
    for k in range(1, n_tp):
        pl.semaphore_signal(barrier, inc=1, device_id={"tp": lax.rem(tp + k, n_tp)})
    for load in loads[:6]:
        load.wait()

    length, channels = x_ref.shape
    groups, states = decay_ref.shape[1:]
    width = groups * states
    each = channels // groups
    steps = length // segments
    order = iota((length, length), 0)
    place = iota((length, length), 1)
    shuffle = (place == (order % segments) * steps + order // segments).astype(f32)
    x = jnp.dot(shuffle.astype(bf16), x_ref[...], preferred_element_type=f32)
    spread = (iota((states, width), 1) % states == iota((states, width), 0)).astype(f32)
    own = iota((groups, width), 1) // states == iota((groups, width), 0)
    diagonal = iota((channels, width), 1) // states == iota((channels, width), 0) // each

    def row(values):
        wide = exact_dot(values, spread)
        return jnp.sum(jnp.where(own, wide, 0.0), axis=0, keepdims=True)

    def table(values):
        return jnp.where(diagonal, exact_dot(values, spread), 0.0)

    gate[...] = exact_dot(exact_dot(shuffle, jnp.exp(gate_ref[...])), own.astype(f32))
    turn_rows = []
    for k in range(2):
        rate = decay_ref[k]
        turn = turn_ref[k]
        retain = jnp.exp(-rate)
        scale = row(jnp.sqrt(1.0 - jnp.exp(-2.0 * rate)))
        turn_rows.append((row(retain * jnp.cos(turn)), row(retain * jnp.sin(turn))))
        push[2 * k] = exact_dot(x, table(drive_re[k]) * scale)
        push[2 * k + 1] = exact_dot(x, table(drive_im[k]) * scale)
    (f_re, f_im), (b_re, b_im) = turn_rows

    zero = jnp.zeros((segments, width), f32)
    one = jnp.ones((segments, width), f32)

    def rows_of(j):
        return pl.ds(pl.multiple_of(j * segments, segments), segments)

    def first(j, c):
        out = []
        for k, (sr, si) in enumerate(((f_re, f_im), (b_re, b_im))):
            at = rows_of(j if k == 0 else steps - 1 - j)
            ar, ai, vr, vi = c[4 * k : 4 * k + 4]
            g = gate[at, :]
            mr, mi = g * sr, g * si
            out += [
                mr * ar - mi * ai,
                mr * ai + mi * ar,
                mr * vr - mi * vi + push[2 * k, at, :],
                mr * vi + mi * vr + push[2 * k + 1, at, :],
            ]
        return tuple(out)

    ends = lax.fori_loop(0, steps, first, (one, zero, zero, zero) * 2)
    for i, part in enumerate(ends):
        seg[i] = part

    def link(parts, c):
        ar, ai, vr, vi = parts
        return (ar * c[0] - ai * c[1] + vr, ar * c[1] + ai * c[0] + vi)

    def seg_rows(k, s):
        return [seg[4 * k + i, s : s + 1, :] for i in range(4)]

    for k in range(2):
        span = range(segments) if k == 0 else range(segments - 1, -1, -1)
        decay = (one[:1], zero[:1])
        state = (zero[:1], zero[:1])
        for s in span:
            parts = seg_rows(k, s)
            state = link(parts, state)
            decay = link(parts[:2] + [0.0, 0.0], decay)
        for i, value in enumerate(decay + state):
            total[4 * k + i : 4 * k + i + 1, :] = value
    totals[sp] = total[...]

    pl.semaphore_wait(barrier, n_sp - 1 + n_tp - 1)

    def hand(k):
        peer = lax.rem(sp + k, n_sp)
        return pltpu.make_async_remote_copy(
            src_ref=total,
            dst_ref=totals.at[sp],
            send_sem=send_a.at[k],
            recv_sem=recv_a.at[sp],
            device_id={"sp": peer},
        )

    def arrival(k):
        source = lax.rem(sp + k, n_sp)
        return pltpu.make_async_remote_copy(
            src_ref=total,
            dst_ref=totals.at[source],
            send_sem=send_a.at[k],
            recv_sem=recv_a.at[source],
            device_id={"sp": source},
        )

    for k in range(1, n_sp):
        hand(k).start()
    for load in loads[6:9]:
        load.wait()
    tables = [(table(read_re[k]), table(read_im[k])) for k in range(2)]
    for k in range(1, n_sp):
        arrival(k).wait_recv()

    for k in range(2):
        c = (zero[:1], zero[:1])
        for d in range(n_sp) if k == 0 else range(n_sp - 1, -1, -1):
            new = link([totals[d, 4 * k + i : 4 * k + i + 1, :] for i in range(4)], c)
            counts = d < sp if k == 0 else d > sp
            c = tuple(jnp.where(counts, a, b) for a, b in zip(new, c))
        for s in range(segments) if k == 0 else range(segments - 1, -1, -1):
            enter[2 * k, s : s + 1, :] = c[0]
            enter[2 * k + 1, s : s + 1, :] = c[1]
            c = link(seg_rows(k, s), c)

    def second(j, c):
        out = []
        for k, (sr, si) in enumerate(((f_re, f_im), (b_re, b_im))):
            at = rows_of(j if k == 0 else steps - 1 - j)
            vr, vi = c[2 * k : 2 * k + 2]
            g = gate[at, :]
            mr, mi = g * sr, g * si
            new_re = mr * vr - mi * vi + push[2 * k, at, :]
            new_im = mr * vi + mi * vr + push[2 * k + 1, at, :]
            push[2 * k, at, :] = new_re
            push[2 * k + 1, at, :] = new_im
            out += [new_re, new_im]
        return tuple(out)

    lax.fori_loop(0, steps, second, tuple(enter[i] for i in range(4)))
    over = ((1,), (1,))
    readout = exact_dot(push[0], tables[0][0], over) - exact_dot(push[1], tables[0][1], over)
    readout = readout + (
        exact_dot(push[2], tables[1][0], over) - exact_dot(push[3], tables[1][1], over)
    )
    readout = readout + skip_ref[...] * x
    mixed = jax.nn.gelu(readout).astype(bf16)
    act[...] = lax.dot_general(
        shuffle.astype(bf16), mixed, (((0,), (0,)), ((), ())), preferred_element_type=f32
    ).astype(bf16)

    share = length // n_tp

    def shift(k, out):
        peer = lax.rem(tp + k, n_tp)
        return pltpu.make_async_remote_copy(
            src_ref=act.at[pl.ds(pl.multiple_of(peer * share, share), share)],
            dst_ref=chan.at[tp if out else peer],
            send_sem=send_b.at[k],
            recv_sem=recv_b.at[tp if out else peer],
            device_id={"tp": peer},
        )

    for k in range(1, n_tp):
        shift(k, True).start()
    chan[tp] = act[pl.ds(pl.multiple_of(tp * share, share), share), :]
    for load in loads[9:]:
        load.wait()
    for k in range(1, n_tp):
        shift(k, False).wait_recv()
    whole = jnp.concatenate([chan[m] for m in range(n_tp)], axis=1)
    branch = jnp.dot(whole, weight[...], preferred_element_type=f32)
    middle_ref[...] = layer_norm(
        deep_alpha * residual_ref[...].astype(f32) + branch, gain_ref[...]
    )
    for k in range(1, n_sp):
        hand(k).wait_send()
    for k in range(1, n_tp):
        shift(k, True).wait_send()


def mixer(args, n_sp, n_tp):
    (residual, x, log_gate, decay, turn, d_re, d_im, r_re, r_im, skip, weight, gain) = args
    length, channels = x.shape
    groups, states = decay.shape[1:]
    width = groups * states
    share, model = residual.shape
    flat = lambda a: a.reshape(2, channels, states)
    operands = (x, log_gate, decay, turn, flat(d_re), flat(d_im), flat(r_re), flat(r_im))
    operands += (skip[None, :], residual, gain[None, :], weight)
    vmem = pl.BlockSpec(memory_space=pltpu.VMEM)
    dma = pltpu.SemaphoreType.DMA
    return pl.pallas_call(
        functools.partial(mixer_kernel, n_sp, n_tp),
        out_shape=jax.ShapeDtypeStruct((share, model), f32),
        in_specs=[pl.BlockSpec(memory_space=pl.ANY)] * len(operands),
        out_specs=vmem,
        scratch_shapes=[pltpu.VMEM(a.shape, a.dtype) for a in operands]
        + [
            pltpu.VMEM((4, length, width), f32),
            pltpu.VMEM((length, width), f32),
            pltpu.VMEM((8, segments, width), f32),
            pltpu.VMEM((4, segments, width), f32),
            pltpu.VMEM((8, width), f32),
            pltpu.VMEM((n_sp, 8, width), f32),
            pltpu.VMEM((length, channels), bf16),
            pltpu.VMEM((n_tp, share, channels), bf16),
            dma((len(operands),)),
            dma((n_sp,)),
            dma((n_sp,)),
            dma((n_tp,)),
            dma((n_tp,)),
        ],
        compiler_params=pltpu.CompilerParams(
            collective_id=0, has_side_effects=True, vmem_limit_bytes=60 * 2**20
        ),
        name="mixer",
    )(*operands)


def experts_kernel(
    n_sp,
    n_tp,
    middle_ref,
    meta_ref,
    gain_ref,
    gate_hbm,
    linear_hbm,
    down_hbm,
    out_ref,
    rows_out,
    recv,
    part,
    sib,
    pair,
    peer_sum,
    final,
    back,
    gate_w,
    linear_w,
    down_w,
    weight_sems,
    s1,
    r1,
    s2x,
    s2d,
    r2,
    s3,
    r3,
    s4,
    r4,
    s5,
    r5,
):
    sp = lax.axis_index("sp")
    tp = lax.axis_index("tp")
    n_hi = n_tp // 2
    hi = tp // 2
    lo = tp % 2
    sibling = hi * 2 + 1 - lo
    barrier = pltpu.get_barrier_semaphore()
    for k in range(1, n_sp):
        pl.semaphore_signal(barrier, inc=1, device_id={"sp": lax.rem(sp + k, n_sp)})
    for k in range(1, n_tp):
        pl.semaphore_signal(barrier, inc=1, device_id={"tp": lax.rem(tp + k, n_tp)})
    fetches = [
        pltpu.make_async_copy(gate_hbm.at[0], gate_w, weight_sems.at[0]),
        pltpu.make_async_copy(linear_hbm.at[0], linear_w, weight_sems.at[1]),
        pltpu.make_async_copy(down_hbm.at[0], down_w, weight_sems.at[2]),
    ]
    for fetch in fetches:
        fetch.start()

    share, model = middle_ref.shape
    length = meta_ref.shape[0]
    slots = rows_out.shape[1]
    room = -(-slots // 8) * 8
    pick = (iota((length, share), 0) == tp * share + iota((length, share), 1)).astype(f32)
    facts = exact_dot(meta_ref[...], pick, ((0,), (0,)))
    expert = iota((n_sp, share), 0).astype(f32)
    first, second = facts[0:1] == expert, facts[1:2] == expert
    uses = jnp.where(first, 1.0, 0.0) + jnp.where(second, 1.0, 0.0)
    weights = jnp.where(first, facts[2:3], 0.0) + jnp.where(second, facts[3:4], 0.0)
    before = (iota((share, share), 0) < iota((share, share), 1)).astype(bf16)
    rank = jnp.dot(uses.astype(bf16), before, preferred_element_type=f32)
    slot = iota((room, share), 0).astype(f32)
    chosen = [
        jnp.where(slot == rank[e : e + 1], uses[e : e + 1], 0.0) for e in range(n_sp)
    ]
    weigh = jnp.concatenate([chosen[e] * weights[e : e + 1] for e in range(n_sp)], axis=0)
    chosen = jnp.concatenate(chosen, axis=0).astype(bf16)
    rows = jnp.dot(chosen, middle_ref[...].astype(bf16), preferred_element_type=f32)
    for e in range(n_sp):
        rows_out[e] = rows[e * room : e * room + slots].astype(bf16)

    pl.semaphore_wait(barrier, n_sp - 1 + n_tp - 1)

    def remote(src, dst, send, receive, where):
        return pltpu.make_async_remote_copy(
            src_ref=src, dst_ref=dst, send_sem=send, recv_sem=receive, device_id=where
        )

    def plus(k):
        return lax.rem(sp + k, n_sp)

    def minus(k):
        return lax.rem(sp + n_sp - k, n_sp)

    def up(k):
        return lax.rem(hi + k, n_hi)

    sends = []

    def go(copy):
        copy.start()
        sends.append(copy)

    for k in range(1, n_sp):
        e = plus(k)
        go(remote(rows_out.at[e], recv.at[tp, sp], s1.at[k], r1.at[sp], {"sp": e}))
    recv[tp, sp] = rows_out[sp]

    def landed(m, s, sem):
        remote(rows_out.at[0], recv.at[m, s], s1.at[0], sem, {"sp": plus(1)}).wait_recv()

    def to_sibling(h, s):
        block = recv.at[h * 2 + lo, s]
        go(remote(block, block, s2d.at[h, s], r2.at[h * 2 + lo, s], {"tp": sibling}))

    def pass_own(s):
        for k in range(1, n_hi):
            h = up(k)
            block = recv.at[tp, s]
            go(remote(block, block, s2x.at[h, s], r2.at[tp, s], {"tp": h * 2 + lo}))
        to_sibling(hi, s)

    pass_own(sp)
    for k in range(1, n_sp):
        s = minus(k)
        landed(tp, s, r1.at[s])
        pass_own(s)
    for k in range(1, n_hi):
        h = up(k)
        for j in range(n_sp):
            s = minus(j)
            landed(h * 2 + lo, s, r2.at[h * 2 + lo, s])
            to_sibling(h, s)
    for fetch in fetches:
        fetch.wait()

    def flat(block):
        block = block.astype(f32)
        if room > slots:
            blank = jnp.zeros((n_sp, room - slots, model), f32)
            block = jnp.concatenate([block, blank], axis=1)
        return block.reshape(n_sp * room, model).astype(bf16)

    def compute(g):
        x = flat(recv[g])
        a = jnp.dot(x, gate_w[...], preferred_element_type=f32)
        b = jnp.dot(x, linear_w[...], preferred_element_type=f32)
        hidden = (jax.nn.silu(a) * b).astype(bf16)
        y = jnp.dot(hidden, down_w[...], preferred_element_type=f32)
        part[g] = y.reshape(n_sp, room, model)[:, :slots].astype(bf16)

    def give(h):
        go(remote(part.at[h * 2 + 1 - lo], sib.at[h], s3.at[h], r3.at[h], {"tp": sibling}))

    def given(h):
        remote(part.at[0], sib.at[h], s3.at[h], r3.at[h], {"tp": sibling}).wait_recv()

    compute(tp)
    for j in range(n_sp):
        s = minus(j)
        landed(sibling, s, r2.at[sibling, s])
    compute(sibling)
    give(hi)
    for k in range(1, n_hi):
        h = up(k)
        other = h * 2 + 1 - lo
        for j in range(n_sp):
            s = minus(j)
            landed(other, s, r2.at[other, s])
        compute(other)
        give(h)
        compute(h * 2 + lo)
        given(h)
        for j in range(n_sp):
            s = plus(j)
            pair[h, s] = (part[h * 2 + lo, s].astype(f32) + sib[h, s].astype(f32)).astype(bf16)
            go(
                remote(
                    pair.at[h, s],
                    peer_sum.at[hi, s],
                    s4.at[h, s],
                    r4.at[hi, s],
                    {"tp": h * 2 + lo},
                )
            )
    given(hi)
    for j in range(n_sp):
        s = plus(j)
        value = part[tp, s].astype(f32) + sib[hi, s].astype(f32)
        for k in range(1, n_hi):
            h = up(k)
            remote(
                pair.at[0, 0], peer_sum.at[h, s], s4.at[0, 0], r4.at[h, s], {"tp": sibling}
            ).wait_recv()
            value = value + peer_sum[h, s].astype(f32)
        if j == 0:
            back[sp] = value.astype(bf16)
        else:
            final[s] = value.astype(bf16)
            go(remote(final.at[s], back.at[sp], s5.at[j], r5.at[sp], {"sp": s}))
    coarse = weigh.astype(bf16)
    fine = (weigh - coarse.astype(f32)).astype(bf16)
    for j in range(1, n_sp):
        s = minus(j)
        remote(final.at[0], back.at[s], s5.at[0], r5.at[s], {"sp": plus(1)}).wait_recv()
    answers = flat(back[...])
    over = (((0,), (0,)), ((), ()))
    routed = lax.dot_general(coarse, answers, over, preferred_element_type=f32)
    routed = routed + lax.dot_general(fine, answers, over, preferred_element_type=f32)
    out_ref[...] = layer_norm(deep_alpha * middle_ref[...] + routed, gain_ref[...]).astype(bf16)
    for copy in sends:
        copy.wait_send()


def experts_layer(middle, meta, gain, gate_weight, linear_weight, down_weight, n_sp, n_tp, slots):
    share, model = middle.shape
    hidden = gate_weight.shape[2]
    n_hi = n_tp // 2
    vmem = pl.BlockSpec(memory_space=pltpu.VMEM)
    hbm = pl.BlockSpec(memory_space=pl.ANY)
    dma = pltpu.SemaphoreType.DMA
    block = (n_sp, slots, model)
    return pl.pallas_call(
        functools.partial(experts_kernel, n_sp, n_tp),
        out_shape=jax.ShapeDtypeStruct((share, model), bf16),
        in_specs=[vmem] * 3 + [hbm] * 3,
        out_specs=vmem,
        scratch_shapes=[
            pltpu.VMEM(block, bf16),
            pltpu.VMEM((n_tp,) + block, bf16),
            pltpu.VMEM((n_tp,) + block, bf16),
            pltpu.VMEM((n_hi,) + block, bf16),
            pltpu.VMEM((n_hi,) + block, bf16),
            pltpu.VMEM((n_hi,) + block, bf16),
            pltpu.VMEM(block, bf16),
            pltpu.VMEM(block, bf16),
            pltpu.VMEM((model, hidden), bf16),
            pltpu.VMEM((model, hidden), bf16),
            pltpu.VMEM((hidden, model), bf16),
            dma((3,)),
            dma((n_sp,)),
            dma((n_sp,)),
            dma((n_hi, n_sp)),
            dma((n_hi, n_sp)),
            dma((n_tp, n_sp)),
            dma((n_hi,)),
            dma((n_hi,)),
            dma((n_hi, n_sp)),
            dma((n_hi, n_sp)),
            dma((n_sp,)),
            dma((n_sp,)),
        ],
        compiler_params=pltpu.CompilerParams(
            collective_id=1, has_side_effects=True, vmem_limit_bytes=60 * 2**20
        ),
        name="experts",
    )(middle, meta, gain[None, :], gate_weight, linear_weight, down_weight)


def on_device(
    residual,
    mixer_input,
    log_gate,
    decay_rate,
    turn_rate,
    drive_real,
    drive_imaginary,
    read_real,
    read_imaginary,
    skip_gain,
    project_weight,
    norm_gain,
    final_gain,
    routes,
    group_weight,
    expert_weight,
    gate_weight,
    linear_weight,
    down_weight,
):
    experts = lax.axis_size("sp")
    members = lax.axis_size("tp")
    middle = mixer(
        (
            residual,
            mixer_input,
            log_gate,
            decay_rate,
            turn_rate,
            drive_real,
            drive_imaginary,
            read_real,
            read_imaginary,
            skip_gain,
            project_weight,
            norm_gain,
        ),
        experts,
        members,
    )
    share = residual.shape[0]
    top = routes.shape[1]
    slots = max(2, 3 * share * top // (2 * experts))
    mixing = group_weight[:, None] * expert_weight / jnp.sum(expert_weight, axis=1, keepdims=True)
    meta = jnp.concatenate([routes.astype(f32), mixing], axis=1)
    return experts_layer(
        middle,
        meta,
        final_gain,
        gate_weight,
        linear_weight,
        down_weight,
        experts,
        members,
        slots,
    )


def solution(mesh):
    placed = (
        P(("sp", "tp"), None),
        P("sp", "tp"),
        P("sp", "tp"),
        P(None, "tp", None),
        P(None, "tp", None),
        P(None, "tp", None, None),
        P(None, "tp", None, None),
        P(None, "tp", None, None),
        P(None, "tp", None, None),
        P("tp"),
        P(),
        P(),
        P(),
        P("sp", None),
        P("sp"),
        P("sp", None),
        P("sp", None, "tp"),
        P("sp", None, "tp"),
        P("sp", "tp", None),
    )
    return jax.shard_map(
        on_device, mesh=mesh, in_specs=placed, out_specs=P(("sp", "tp"), None), check_vma=False
    )
```

profile of v0, /device:TPU:13, one launch (start us, length us, event | category | flops | bytes accessed | tf_op | source)
XLA Modules:
  0.0 87.3 jit_solution(11728269479849495130)
XLA Ops:
  0.0 0.7 reduce_sum.9
  0.7 0.7 multiply_divide_fusion
  1.4 0.7 convert_element_type.3
  2.1 0.8 copy.26.meta_ref
  2.9 1.5 %copy.25.refs_1_ = f32[192,8]{1,0:T(8,128)} copy(f32[192,8]{0,1:T(8,128)} %param.21) | data formatting | bytes 12288 | tf_op args[2]
  4.3 18.1 %mixer.1.middle_ref = f32[48,2048]{1,0:T(8,128)} custom-call(bf16[192,128]{1,0:T(8,128)(2,1)} %refs_0_.1, f32[192,8]{1,0:T(8,128)} %copy.25.refs_1_, f32[2,8,64]{2,1,0:T(8,128)} %refs_2_.1, f32[2,8,64]{2,1,0:T(8,128)} %refs_3_.1, f32[2,128,64]{2,1,0:T(8,128)} %bitcast.7, f32[2,128,64]{2,1,0:T(8,128)} %bitcast.8, f32[2,128,64]{2,1,0:T(8,128)} %bitcast.9, ...), custom_call_target="tpu_custom_call" | custom-call | tf_op jit(solution)/shard_map/mixer/pallas_call | solution.py:238
  22.5 63.1 %experts.1 = bf16[48,2048]{1,0:T(8,128)(2,1)} custom-call(f32[48,2048]{1,0:T(8,128)} %mixer.1.middle_ref, f32[192,4]{1,0:T(8,128)} %copy.26.meta_ref, f32[1,2048]{1,0:T(1,128)} %bitcast.12, bf16[1,2048,256]{2,1,0:T(8,128)(2,1)} %gate_hbm.1, bf16[1,2048,256]{2,1,0:T(8,128)(2,1)} %linear_hbm.1, bf16[1,256,2048]{2,1,0:T(8,128)(2,1)} %down_hbm.1), custom_call_target="tpu_custom_call" | custom-call | tf_op jit(solution)/shard_map/experts/pallas_call | solution.py:482
  85.6 1.6 %copy.28 = bf16[48,2048]{1,0:T(8,128)(2,1)} copy(bf16[48,2048]{1,0:T(8,128)(2,1)} %experts.1) | data formatting | bytes 393216
  (1 shorter events, 0.0 us)
where the time goes:
time: 87.5 us; the launch traced here: 87.3 us
  Pallas kernels  81.3 us (93%)
  local copies, waits for them, and re-layouts  3.84 us (4%)
  other arithmetic  2.1 us (2%)
    pallas_call x1, Pallas kernels, experts_layer(): pl.pallas_call(functools.partial(experts_kernel, n_sp, n_tp), out_shape=j...  63.1 us
    pallas_call x1, Pallas kernels, mixer(): pl.pallas_call(functools.partial(mixer_kernel, n_sp, n_tp), out_shape=jax...  18.1 us
    unnamed x2, local copies, waits for them, and re-layouts  3.07 us

commit v1 on v0

v1 whole, which is shorter than its diff:
```python
import functools

import jax
import jax.numpy as jnp
from jax import lax
from jax.experimental import pallas as pl
from jax.experimental.pallas import tpu as pltpu
from jax.sharding import PartitionSpec as P

deep_alpha = 2.0**0.25
norm_epsilon = 1e-05
highest = lax.Precision.HIGHEST
f32 = jnp.float32
bf16 = jnp.bfloat16
segments = 8


def layer_norm(values, gain):
    center = values - jnp.mean(values, axis=-1, keepdims=True)
    spread = jnp.mean(center * center, axis=-1, keepdims=True)
    return center * lax.rsqrt(spread + norm_epsilon) * gain


def iota(shape, axis):
    return lax.broadcasted_iota(jnp.int32, shape, axis)


def exact_dot(a, b, dims=((1,), (0,))):
    return lax.dot_general(a, b, (dims, ((), ())), precision=highest, preferred_element_type=f32)


def mixer_body(n_sp, n_tp, early, linked, sends, refs):
    sources, staged = refs[:12], refs[12:24]
    (push, gate, seg, enter, total, totals, act, chan) = refs[24:32]
    (stage_sems, send_a, recv_a, send_b, recv_b) = refs[32:]
    loads = [
        pltpu.make_async_copy(source, place, stage_sems.at[i])
        for i, (source, place) in enumerate(zip(sources, staged))
    ]
    for load in loads:
        load.start()
    early()
    (x_ref, gate_ref, decay_ref, turn_ref, drive_re, drive_im) = staged[:6]
    (read_re, read_im, skip_ref, residual_ref, gain_ref, weight) = staged[6:]
    sp = lax.axis_index("sp")
    tp = lax.axis_index("tp")
    barrier = pltpu.get_barrier_semaphore()
    for k in range(1, n_sp):
        pl.semaphore_signal(barrier, inc=1, device_id={"sp": lax.rem(sp + k, n_sp)})
    for k in range(1, n_tp):
        pl.semaphore_signal(barrier, inc=1, device_id={"tp": lax.rem(tp + k, n_tp)})
    for load in loads[:6]:
        load.wait()

    length, channels = x_ref.shape
    groups, states = decay_ref.shape[1:]
    width = groups * states
    each = channels // groups
    steps = length // segments
    order = iota((length, length), 0)
    place = iota((length, length), 1)
    shuffle = (place == (order % segments) * steps + order // segments).astype(f32)
    x = jnp.dot(shuffle.astype(bf16), x_ref[...], preferred_element_type=f32)
    spread = (iota((states, width), 1) % states == iota((states, width), 0)).astype(f32)
    own = iota((groups, width), 1) // states == iota((groups, width), 0)
    diagonal = iota((channels, width), 1) // states == iota((channels, width), 0) // each

    def row(values):
        wide = exact_dot(values, spread)
        return jnp.sum(jnp.where(own, wide, 0.0), axis=0, keepdims=True)

    def table(values):
        return jnp.where(diagonal, exact_dot(values, spread), 0.0)

    gates = exact_dot(shuffle, jnp.exp(gate_ref[...]), ((1,), (1,)))
    gate[...] = exact_dot(gates, own.astype(f32))
    turn_rows = []
    for k in range(2):
        rate = decay_ref[k]
        turn = turn_ref[k]
        retain = jnp.exp(-rate)
        scale = row(jnp.sqrt(1.0 - jnp.exp(-2.0 * rate)))
        turn_rows.append((row(retain * jnp.cos(turn)), row(retain * jnp.sin(turn))))
        push[2 * k] = exact_dot(x, table(drive_re[k]) * scale)
        push[2 * k + 1] = exact_dot(x, table(drive_im[k]) * scale)
    (f_re, f_im), (b_re, b_im) = turn_rows

    zero = jnp.zeros((segments, width), f32)
    one = jnp.ones((segments, width), f32)

    def rows_of(j):
        return pl.ds(pl.multiple_of(j * segments, segments), segments)

    def first(j, c):
        out = []
        for k, (sr, si) in enumerate(((f_re, f_im), (b_re, b_im))):
            at = rows_of(j if k == 0 else steps - 1 - j)
            ar, ai, vr, vi = c[4 * k : 4 * k + 4]
            g = gate[at, :]
            mr, mi = g * sr, g * si
            out += [
                mr * ar - mi * ai,
                mr * ai + mi * ar,
                mr * vr - mi * vi + push[2 * k, at, :],
                mr * vi + mi * vr + push[2 * k + 1, at, :],
            ]
        return tuple(out)

    ends = lax.fori_loop(0, steps, first, (one, zero, zero, zero) * 2)
    for i, part in enumerate(ends):
        seg[i] = part

    def link(parts, c):
        ar, ai, vr, vi = parts
        return (ar * c[0] - ai * c[1] + vr, ar * c[1] + ai * c[0] + vi)

    def seg_rows(k, s):
        return [seg[4 * k + i, s : s + 1, :] for i in range(4)]

    for k in range(2):
        span = range(segments) if k == 0 else range(segments - 1, -1, -1)
        decay = (one[:1], zero[:1])
        state = (zero[:1], zero[:1])
        for s in span:
            parts = seg_rows(k, s)
            state = link(parts, state)
            decay = link(parts[:2] + [0.0, 0.0], decay)
        for i, value in enumerate(decay + state):
            total[4 * k + i : 4 * k + i + 1, :] = value
    totals[sp] = total[...]

    pl.semaphore_wait(barrier, n_sp - 1 + n_tp - 1)

    def hand(k):
        peer = lax.rem(sp + k, n_sp)
        return pltpu.make_async_remote_copy(
            src_ref=total,
            dst_ref=totals.at[sp],
            send_sem=send_a.at[k],
            recv_sem=recv_a.at[sp],
            device_id={"sp": peer},
        )

    def arrival(k):
        source = lax.rem(sp + k, n_sp)
        return pltpu.make_async_remote_copy(
            src_ref=total,
            dst_ref=totals.at[source],
            send_sem=send_a.at[k],
            recv_sem=recv_a.at[source],
            device_id={"sp": source},
        )

    for k in range(1, n_sp):
        sends.append(hand(k))
        sends[-1].start()
    linked()
    for load in loads[6:9]:
        load.wait()
    tables = [(table(read_re[k]), table(read_im[k])) for k in range(2)]
    for k in range(1, n_sp):
        arrival(k).wait_recv()

    for k in range(2):
        c = (zero[:1], zero[:1])
        for d in range(n_sp) if k == 0 else range(n_sp - 1, -1, -1):
            new = link([totals[d, 4 * k + i : 4 * k + i + 1, :] for i in range(4)], c)
            counts = d < sp if k == 0 else d > sp
            c = tuple(jnp.where(counts, a, b) for a, b in zip(new, c))
        for s in range(segments) if k == 0 else range(segments - 1, -1, -1):
            enter[2 * k, s : s + 1, :] = c[0]
            enter[2 * k + 1, s : s + 1, :] = c[1]
            c = link(seg_rows(k, s), c)

    def second(j, c):
        out = []
        for k, (sr, si) in enumerate(((f_re, f_im), (b_re, b_im))):
            at = rows_of(j if k == 0 else steps - 1 - j)
            vr, vi = c[2 * k : 2 * k + 2]
            g = gate[at, :]
            mr, mi = g * sr, g * si
            new_re = mr * vr - mi * vi + push[2 * k, at, :]
            new_im = mr * vi + mi * vr + push[2 * k + 1, at, :]
            push[2 * k, at, :] = new_re
            push[2 * k + 1, at, :] = new_im
            out += [new_re, new_im]
        return tuple(out)

    lax.fori_loop(0, steps, second, tuple(enter[i] for i in range(4)))
    over = ((1,), (1,))
    readout = exact_dot(push[0], tables[0][0], over) - exact_dot(push[1], tables[0][1], over)
    readout = readout + (
        exact_dot(push[2], tables[1][0], over) - exact_dot(push[3], tables[1][1], over)
    )
    readout = readout + skip_ref[...] * x
    mixed = jax.nn.gelu(readout).astype(bf16)
    act[...] = lax.dot_general(
        shuffle.astype(bf16), mixed, (((0,), (0,)), ((), ())), preferred_element_type=f32
    ).astype(bf16)

    share = length // n_tp

    def shift(k, out):
        peer = lax.rem(tp + k, n_tp)
        return pltpu.make_async_remote_copy(
            src_ref=act.at[pl.ds(pl.multiple_of(peer * share, share), share)],
            dst_ref=chan.at[tp if out else peer],
            send_sem=send_b.at[k],
            recv_sem=recv_b.at[tp if out else peer],
            device_id={"tp": peer},
        )

    for k in range(1, n_tp):
        sends.append(shift(k, True))
        sends[-1].start()
    chan[tp] = act[pl.ds(pl.multiple_of(tp * share, share), share), :]
    for load in loads[9:]:
        load.wait()
    for k in range(1, n_tp):
        shift(k, False).wait_recv()
    whole = jnp.concatenate([chan[m] for m in range(n_tp)], axis=1)
    branch = jnp.dot(whole, weight[...], preferred_element_type=f32)
    return layer_norm(deep_alpha * residual_ref[...].astype(f32) + branch, gain_ref[...])


def flip(base, k):
    out, bit = base, 1
    while bit <= k:
        if k & bit:
            out = out + bit - 2 * bit * lax.rem(lax.div(base, bit), 2)
        bit *= 2
    return out


def shape_of_block(slots, model):
    while slots % 16 == 0 or 16 % (slots % 16):
        slots += 1
    main, extra = slots // 16, slots % 16
    fold = 16 // extra
    return main, extra, fold, model // fold


def layer_kernel(n_sp, n_tp, slots, *refs):
    mixer_in, refs = refs[:12], refs[12:]
    small_in, refs = refs[:4], refs[4:]
    (gate_hbm, linear_hbm, down_hbm, out_ref), refs = refs[:4], refs[4:]
    mixer_scratch, refs = refs[:25], refs[25:]
    small, refs = refs[:4], refs[4:]
    (middle_ref, rows_out, recv, own, part, got, final, back), refs = refs[:8], refs[8:]
    (gate_w, linear_w, down_w), refs = refs[:3], refs[3:]
    (small_sems, weight_sems, give_sems, take_sems), refs = refs[:4], refs[4:]
    s1, r1, s2, r2, s3, r3, s4, r4 = refs

    sp = lax.axis_index("sp")
    tp = lax.axis_index("tp")
    n_hi = n_tp // 2
    hi = lax.div(tp, 2)
    lo = lax.rem(tp, 2)
    sibling = {"tp": hi * 2 + 1 - lo}
    sends = []

    def remote(src, dst, send, receive, where):
        return pltpu.make_async_remote_copy(
            src_ref=src, dst_ref=dst, send_sem=send, recv_sem=receive, device_id=where
        )

    def go(copy):
        copy.start()
        sends.append(copy)

    width = gate_hbm.shape[2]
    homes = [(gate_hbm, gate_w.at[0]), (linear_hbm, linear_w.at[0]), (down_hbm, down_w.at[0:width])]
    others = [gate_w.at[1], linear_w.at[1], down_w.at[width : 2 * width]]
    fetches = [
        pltpu.make_async_copy(source.at[0], place, weight_sems.at[i])
        for i, (source, place) in enumerate(homes)
    ]
    swaps = [
        remote(homes[i][0].at[0], others[i], give_sems.at[i], take_sems.at[i], sibling)
        for i in range(3)
    ]
    stages = [
        pltpu.make_async_copy(source, place, small_sems.at[i])
        for i, (source, place) in enumerate(zip(small_in, small))
    ]

    def early():
        for copy in stages + fetches:
            copy.start()

    def linked():
        for copy in swaps:
            go(copy)

    middle = mixer_body(n_sp, n_tp, early, linked, sends, mixer_in + mixer_scratch)
    middle_ref[...] = middle
    for copy in stages:
        copy.wait()
    routes_ref, group_ref, shares_ref, gain_ref = small

    share, model = middle.shape
    length = routes_ref.shape[1]
    main, extra, fold, piece = shape_of_block(slots, model)
    per = 16 * main + 16
    line = iota((16, piece), 0) % fold
    masks = [line == c for c in range(fold)]
    keep = [mask.astype(f32).astype(bf16) for mask in masks]

    weights = shares_ref[...]
    weights = group_ref[...] * weights / jnp.sum(weights, axis=0, keepdims=True)
    table = jnp.concatenate([routes_ref[...].astype(f32), weights], axis=0)
    pick = (iota((length, share), 0) == tp * share + iota((length, share), 1)).astype(f32)
    facts = exact_dot(table, pick)
    peers = [flip(sp, k) for k in range(n_sp)]
    expert = lax.bitwise_xor(iota((n_sp, share), 0), jnp.full((n_sp, share), sp, jnp.int32))
    expert = expert.astype(f32)
    first, second = facts[0:1] == expert, facts[1:2] == expert
    uses = jnp.where(first, 1.0, 0.0) + jnp.where(second, 1.0, 0.0)
    amounts = jnp.where(first, facts[2:3], 0.0) + jnp.where(second, facts[3:4], 0.0)
    before = (iota((share, share), 0) < iota((share, share), 1)).astype(bf16)
    rank = jnp.dot(uses.astype(bf16), before, preferred_element_type=f32)
    place = iota((per, share), 0)
    slot = jnp.where(place < 16 * main, place, 16 * main + (place - 16 * main) // fold)
    slot = slot.astype(f32)
    chosen = [
        jnp.where(slot == rank[k : k + 1], uses[k : k + 1], 0.0) for k in range(n_sp)
    ]
    weigh = jnp.concatenate([chosen[k] * amounts[k : k + 1] for k in range(n_sp)], axis=0)
    weigh = weigh.T
    coarse = weigh.astype(bf16)
    fine = (weigh - coarse.astype(f32)).astype(bf16)
    weigh = jnp.concatenate([coarse, fine], axis=0)

    def pack(values, extras, store):
        for i in range(main):
            store(slice(i * model, (i + 1) * model), values[16 * i : 16 * i + 16])
        folded = jnp.where(masks[0], extras[:, :piece], 0.0)
        for c in range(1, fold):
            folded = jnp.where(masks[c], extras[:, c * piece : (c + 1) * piece], folded)
        store(slice(main * model, main * model + piece), folded)

    def unpack(block):
        mains = [block[:, i * model : (i + 1) * model] for i in range(main)]
        tail = block[:, main * model :]
        return mains, jnp.concatenate([tail * keep[c] for c in range(fold)], axis=1)

    rows = jnp.dot(
        jnp.concatenate(chosen, axis=0).astype(bf16),
        middle.astype(bf16),
        preferred_element_type=f32,
    )
    for k in range(n_sp):
        block = rows[k * per : (k + 1) * per]

        def store(columns, values):
            rows_out[k, :, columns] = values.astype(bf16)

        pack(block, block[16 * main :], store)

    def across(j):
        return {"tp": flip(hi, j) * 2 + lo}

    def relay(k):
        if k:
            remote(rows_out.at[k], recv.at[0, k], s1.at[k], r1.at[k], {"sp": peers[k]}).wait_recv()
        source = recv.at[0, k] if k else rows_out.at[0]
        for j in range(1, n_hi):
            go(remote(source, recv.at[j, k], s2.at[j, k], r2.at[j, k], across(j)))

    def compute(ks):
        blocks = [(j, k) for k in ks for j in range(n_hi)]
        mains, extras = [], []
        for j, k in blocks:
            if j:
                remote(
                    recv.at[0, k], recv.at[j, k], s2.at[j, k], r2.at[j, k], across(j)
                ).wait_recv()
            a, b = unpack(recv[j, k] if j or k else rows_out[0])
            mains += a
            extras.append(b)
        x = jnp.concatenate(mains + extras, axis=0)
        count = 16 * len(mains)

        def project(weight):
            value = jnp.concatenate(
                [jnp.dot(x, weight[i], preferred_element_type=f32) for i in range(2)], axis=1
            )
            tail = value[count:].reshape(len(blocks) * extra, fold, 2 * width)
            tail = jnp.sum(tail, axis=1, keepdims=True)
            tail = jnp.broadcast_to(tail, (len(blocks) * extra, fold, 2 * width))
            tail = tail.reshape(len(blocks) * 16, 2 * width)
            return jnp.concatenate([value[:count], tail], axis=0) if count else tail

        hidden = (jax.nn.silu(project(gate_w)) * project(linear_w)).astype(bf16)
        y = jnp.dot(hidden, down_w[...], preferred_element_type=f32)
        for i, (j, k) in enumerate(blocks):

            def store(columns, values):
                if j:
                    part[j, k, :, columns] = values.astype(bf16)
                else:
                    own[k, :, columns] = values

            pack(
                y[16 * main * i : 16 * main * (i + 1)],
                y[count + 16 * i : count + 16 * i + 16],
                store,
            )
            if j:
                go(remote(part.at[j, k], got.at[j, k], s3.at[j, k], r3.at[j, k], across(j)))

    def combine(k):
        value = own[k]
        for j in range(1, n_hi):
            remote(part.at[j, k], got.at[j, k], s3.at[j, k], r3.at[j, k], across(j)).wait_recv()
            value = value + got[j, k].astype(f32)
        if k:
            final[k] = value.astype(bf16)
            go(remote(final.at[k], back.at[k], s4.at[k], r4.at[k], {"sp": peers[k]}))
        else:
            back[0] = value.astype(bf16)

    for k in range(1, n_sp):
        go(remote(rows_out.at[k], recv.at[0, k], s1.at[k], r1.at[k], {"sp": peers[k]}))
    unit = max(1, n_sp // 8)
    rounds = [range(i, i + unit) for i in range(0, n_sp, unit)]
    ahead, behind = 1, 2
    for ks in rounds[:ahead]:
        for k in ks:
            relay(k)
    for fetch in fetches:
        fetch.wait()
    for i in range(len(rounds) + behind):
        for k in rounds[i + ahead] if i + ahead < len(rounds) else ():
            relay(k)
        if i == 0:
            for copy in swaps:
                copy.wait_recv()
        if i < len(rounds):
            compute(rounds[i])
        for k in rounds[i - behind] if i >= behind else ():
            combine(k)

    answers = []
    for k in range(n_sp):
        if k:
            remote(final.at[k], back.at[k], s4.at[k], r4.at[k], {"sp": peers[k]}).wait_recv()
        mains, tail = unpack(back[k])
        answers += mains + [tail]
    routed = jnp.dot(weigh, jnp.concatenate(answers, axis=0), preferred_element_type=f32)
    routed = routed[:share] + routed[share:]
    out_ref[...] = layer_norm(deep_alpha * middle_ref[...] + routed, gain_ref[...]).astype(bf16)
    for copy in sends:
        copy.wait_send()


def on_device(
    residual,
    mixer_input,
    log_gate,
    decay_rate,
    turn_rate,
    drive_real,
    drive_imaginary,
    read_real,
    read_imaginary,
    skip_gain,
    project_weight,
    norm_gain,
    final_gain,
    routes,
    group_weight,
    expert_weight,
    gate_weight,
    linear_weight,
    down_weight,
):
    n_sp = lax.axis_size("sp")
    n_tp = lax.axis_size("tp")
    n_hi = n_tp // 2
    length, channels = mixer_input.shape
    groups, states = decay_rate.shape[1:]
    width = groups * states
    share, model = residual.shape
    hidden = gate_weight.shape[2]
    top = routes.shape[1]
    slots = max(2, 3 * share * top // (2 * n_sp))
    main, extra, fold, piece = shape_of_block(slots, model)
    flat = lambda a: a.reshape(2, channels, states)
    staged = (mixer_input, log_gate.T, decay_rate, turn_rate)
    staged += tuple(flat(a) for a in (drive_real, drive_imaginary, read_real, read_imaginary))
    staged += (skip_gain[None, :], residual, norm_gain[None, :], project_weight)
    small = (routes.T, group_weight[None, :], expert_weight.T, final_gain[None, :])
    operands = staged + small + (gate_weight, linear_weight, down_weight)
    dma = pltpu.SemaphoreType.DMA
    block = (16, main * model + piece)
    return pl.pallas_call(
        functools.partial(layer_kernel, n_sp, n_tp, slots),
        out_shape=jax.ShapeDtypeStruct((share, model), bf16),
        in_specs=[pl.BlockSpec(memory_space=pl.ANY)] * len(operands),
        out_specs=pl.BlockSpec(memory_space=pltpu.VMEM),
        scratch_shapes=[pltpu.VMEM(a.shape, a.dtype) for a in staged]
        + [
            pltpu.VMEM((4, length, width), f32),
            pltpu.VMEM((length, width), f32),
            pltpu.VMEM((8, segments, width), f32),
            pltpu.VMEM((4, segments, width), f32),
            pltpu.VMEM((8, width), f32),
            pltpu.VMEM((n_sp, 8, width), f32),
            pltpu.VMEM((length, channels), bf16),
            pltpu.VMEM((n_tp, share, channels), bf16),
            dma((len(staged),)),
            dma((n_sp,)),
            dma((n_sp,)),
            dma((n_tp,)),
            dma((n_tp,)),
        ]
        + [pltpu.VMEM(a.shape, a.dtype) for a in small]
        + [
            pltpu.VMEM((share, model), f32),
            pltpu.VMEM((n_sp,) + block, bf16),
            pltpu.VMEM((n_hi, n_sp) + block, bf16),
            pltpu.VMEM((n_sp,) + block, f32),
            pltpu.VMEM((n_hi, n_sp) + block, bf16),
            pltpu.VMEM((n_hi, n_sp) + block, bf16),
            pltpu.VMEM((n_sp,) + block, bf16),
            pltpu.VMEM((n_sp,) + block, bf16),
            pltpu.VMEM((2, model, hidden), bf16),
            pltpu.VMEM((2, model, hidden), bf16),
            pltpu.VMEM((2 * hidden, model), bf16),
            dma((len(small),)),
            dma((3,)),
            dma((3,)),
            dma((3,)),
            dma((n_sp,)),
            dma((n_sp,)),
            dma((n_hi, n_sp)),
            dma((n_hi, n_sp)),
            dma((n_hi, n_sp)),
            dma((n_hi, n_sp)),
            dma((n_sp,)),
            dma((n_sp,)),
        ],
        compiler_params=pltpu.CompilerParams(
            collective_id=0, has_side_effects=True, vmem_limit_bytes=60 * 2**20
        ),
        name="layer",
    )(*operands)


def solution(mesh):
    placed = (
        P(("sp", "tp"), None),
        P("sp", "tp"),
        P("sp", "tp"),
        P(None, "tp", None),
        P(None, "tp", None),
        P(None, "tp", None, None),
        P(None, "tp", None, None),
        P(None, "tp", None, None),
        P(None, "tp", None, None),
        P("tp"),
        P(),
        P(),
        P(),
        P("sp", None),
        P("sp"),
        P("sp", None),
        P("sp", None, "tp"),
        P("sp", None, "tp"),
        P("sp", "tp", None),
    )
    return jax.shard_map(
        on_device, mesh=mesh, in_specs=placed, out_specs=P(("sp", "tp"), None), check_vma=False
    )
```

time: 87.5 us -> 61.4 us (0.70)
  the two profiles are of different devices: /device:TPU:13 before, /device:TPU:0 now
where the time goes in v1:
time: 61.4 us; the launch traced here: 61.3 us
  Pallas kernels  59.7 us (97%)
  local copies, waits for them, and re-layouts  1.62 us (3%)
    pallas_call x1, Pallas kernels, on_device(): pl.pallas_call(functools.partial(layer_kernel, n_sp, n_tp, slots), out_sh...  59.7 us
    unnamed x1, local copies, waits for them, and re-layouts  1.62 us

profile of v1, /device:TPU:0, one launch (start us, length us, event | category | flops | bytes accessed | tf_op | source)
XLA Modules:
  0.0 61.3 jit_solution(13358502738985783905)
XLA Ops:
  0.0 59.7 %layer.1 = bf16[48,2048]{1,0:T(8,128)(2,1)} custom-call(bf16[192,128]{1,0:T(8,128)(2,1)} %refs_0_.1, f32[8,192]{1,0:T(8,128)} %bitcast.15, f32[2,8,64]{2,1,0:T(8,128)} %refs_2_.1, f32[2,8,64]{2,1,0:T(8,128)} %refs_3_.1, f32[2,128,64]{2,1,0:T(8,128)} %bitcast.11, f32[2,128,64]{2,1,0:T(8,128)} %bitcast.12, f32[2,128,64]{2,1,0:T(8,128)} %bitcast.13, ...), custom_call_target="tpu_custom_call" | custom-call | tf_op jit(solution)/shard_map/layer/pallas_call | solution.py:497
  59.7 1.6 %copy.21 = bf16[48,2048]{1,0:T(8,128)(2,1)} copy(bf16[48,2048]{1,0:T(8,128)(2,1)} %layer.1) | data formatting | bytes 393216

commit v2 on v1

--- a/solution.py
+++ b/solution.py
@@ -246,10 +246,10 @@
     (gate_hbm, linear_hbm, down_hbm, out_ref), refs = refs[:4], refs[4:]
     mixer_scratch, refs = refs[:25], refs[25:]
     small, refs = refs[:4], refs[4:]
-    (middle_ref, rows_out, recv, own, part, got, final, back), refs = refs[:8], refs[8:]
+    (middle_ref, plain, rows_out, recv, own, part, got, final, back), refs = refs[:9], refs[9:]
     (gate_w, linear_w, down_w), refs = refs[:3], refs[3:]
     (small_sems, weight_sems, give_sems, take_sems), refs = refs[:4], refs[4:]
-    s1, r1, s2, r2, s3, r3, s4, r4 = refs
+    s0, r0, s1, r1, s2, r2, s3, r3, s4, r4 = refs
 
     sp = lax.axis_index("sp")
     tp = lax.axis_index("tp")
@@ -294,6 +294,16 @@
 
     middle = mixer_body(n_sp, n_tp, early, linked, sends, mixer_in + mixer_scratch)
     middle_ref[...] = middle
+    plain[0] = middle.astype(bf16)
+
+    def across(j):
+        return {"tp": flip(hi, j) * 2 + lo}
+
+    def crossing(j):
+        return remote(plain.at[0], plain.at[j], s0.at[j], r0.at[j], across(j))
+
+    for j in range(1, n_hi):
+        go(crossing(j))
     for copy in stages:
         copy.wait()
     routes_ref, group_ref, shares_ref, gain_ref = small
@@ -309,22 +319,39 @@
     weights = shares_ref[...]
     weights = group_ref[...] * weights / jnp.sum(weights, axis=0, keepdims=True)
     table = jnp.concatenate([routes_ref[...].astype(f32), weights], axis=0)
-    pick = (iota((length, share), 0) == tp * share + iota((length, share), 1)).astype(f32)
-    facts = exact_dot(table, pick)
-    peers = [flip(sp, k) for k in range(n_sp)]
-    expert = lax.bitwise_xor(iota((n_sp, share), 0), jnp.full((n_sp, share), sp, jnp.int32))
+    def look(member):
+        pick = (iota((length, share), 0) == member * share + iota((length, share), 1)).astype(f32)
+        return exact_dot(table, pick)
+
+    half = max(1, n_sp // 2)
+    upper = lax.div(sp, half)
+    depth = sp + upper * (n_sp - 1 - 2 * sp)
+
+    def mirrored(index, side):
+        return index + side * (n_sp - 1 - 2 * index)
+
+    peers = [mirrored(flip(depth, k), upper) for k in range(half)]
+    peers += [mirrored(k, 1 - upper) for k in range(n_sp - half)]
+    mine = [k if k < half else half + depth for k in range(n_sp)]
+    expert = jnp.full((n_sp, share), sp, jnp.int32)
+    for k in range(1, n_sp):
+        expert = jnp.where(iota((n_sp, share), 0) == k, peers[k], expert)
     expert = expert.astype(f32)
-    first, second = facts[0:1] == expert, facts[1:2] == expert
-    uses = jnp.where(first, 1.0, 0.0) + jnp.where(second, 1.0, 0.0)
-    amounts = jnp.where(first, facts[2:3], 0.0) + jnp.where(second, facts[3:4], 0.0)
     before = (iota((share, share), 0) < iota((share, share), 1)).astype(bf16)
-    rank = jnp.dot(uses.astype(bf16), before, preferred_element_type=f32)
     place = iota((per, share), 0)
     slot = jnp.where(place < 16 * main, place, 16 * main + (place - 16 * main) // fold)
     slot = slot.astype(f32)
-    chosen = [
-        jnp.where(slot == rank[k : k + 1], uses[k : k + 1], 0.0) for k in range(n_sp)
-    ]
+
+    def choose(facts, count):
+        first, second = facts[0:1] == expert, facts[1:2] == expert
+        uses = jnp.where(first, 1.0, 0.0) + jnp.where(second, 1.0, 0.0)
+        amounts = jnp.where(first, facts[2:3], 0.0) + jnp.where(second, facts[3:4], 0.0)
+        rank = jnp.dot(uses.astype(bf16), before, preferred_element_type=f32)
+        picks = [jnp.where(slot == rank[k : k + 1], uses[k : k + 1], 0.0) for k in range(count)]
+        return picks, amounts
+
+    chosen, amounts = choose(look(tp), n_sp)
+    theirs = [choose(look(across(j)["tp"]), half)[0] for j in range(1, n_hi)]
     weigh = jnp.concatenate([chosen[k] * amounts[k : k + 1] for k in range(n_sp)], axis=0)
     weigh = weigh.T
     coarse = weigh.astype(bf16)
@@ -344,38 +371,38 @@
         tail = block[:, main * model :]
         return mains, jnp.concatenate([tail * keep[c] for c in range(fold)], axis=1)
 
-    rows = jnp.dot(
-        jnp.concatenate(chosen, axis=0).astype(bf16),
-        middle.astype(bf16),
-        preferred_element_type=f32,
-    )
-    for k in range(n_sp):
-        block = rows[k * per : (k + 1) * per]
-
-        def store(columns, values):
-            rows_out[k, :, columns] = values.astype(bf16)
-
-        pack(block, block[16 * main :], store)
-
-    def across(j):
-        return {"tp": flip(hi, j) * 2 + lo}
+    def select(picks, j):
+        picks = jnp.concatenate(picks, axis=0).astype(bf16)
+        rows = jnp.dot(picks, plain[j], preferred_element_type=f32)
+        for k in range(picks.shape[0] // per):
+            block = rows[k * per : (k + 1) * per]
+
+            def store(columns, values):
+                rows_out[j, k, :, columns] = values.astype(bf16)
+
+            pack(block, block[16 * main :], store)
+
+    select(chosen, 0)
+
+    def arrive(k):
+        remote(rows_out.at[0, k], recv.at[0, k], s1.at[k], r1.at[k], {"sp": peers[k]}).wait_recv()
 
     def relay(k):
-        if k:
-            remote(rows_out.at[k], recv.at[0, k], s1.at[k], r1.at[k], {"sp": peers[k]}).wait_recv()
-        source = recv.at[0, k] if k else rows_out.at[0]
+        arrive(k)
         for j in range(1, n_hi):
-            go(remote(source, recv.at[j, k], s2.at[j, k], r2.at[j, k], across(j)))
+            go(remote(recv.at[0, k], recv.at[j, k], s2.at[j, k], r2.at[j, k], across(j)))
 
     def compute(ks):
         blocks = [(j, k) for k in ks for j in range(n_hi)]
         mains, extras = [], []
         for j, k in blocks:
-            if j:
+            if j and k:
                 remote(
                     recv.at[0, k], recv.at[j, k], s2.at[j, k], r2.at[j, k], across(j)
                 ).wait_recv()
-            a, b = unpack(recv[j, k] if j or k else rows_out[0])
+            elif k and k < half:
+                arrive(k)
+            a, b = unpack(recv[j, k] if k else rows_out[j, 0])
             mains += a
             extras.append(b)
         x = jnp.concatenate(mains + extras, axis=0)
@@ -416,30 +443,49 @@
             value = value + got[j, k].astype(f32)
         if k:
             final[k] = value.astype(bf16)
-            go(remote(final.at[k], back.at[k], s4.at[k], r4.at[k], {"sp": peers[k]}))
+            there = mine[k]
+            go(remote(final.at[k], back.at[there], s4.at[k], r4.at[there], {"sp": peers[k]}))
         else:
             back[0] = value.astype(bf16)
 
-    for k in range(1, n_sp):
-        go(remote(rows_out.at[k], recv.at[0, k], s1.at[k], r1.at[k], {"sp": peers[k]}))
     unit = max(1, n_sp // 8)
-    rounds = [range(i, i + unit) for i in range(0, n_sp, unit)]
-    ahead, behind = 1, 2
-    for ks in rounds[:ahead]:
-        for k in ks:
-            relay(k)
+
+    def eighth(i):
+        return range(i * unit, i * unit + unit)
+
+    for i in (0, 1, 4, 6, 5, 7, 2, 3):
+        for k in eighth(i):
+            if k:
+                there = mine[k]
+                go(
+                    remote(
+                        rows_out.at[0, k],
+                        recv.at[0, there],
+                        s1.at[k],
+                        r1.at[there],
+                        {"sp": peers[k]},
+                    )
+                )
+    for j in range(1, n_hi):
+        crossing(j).wait_recv()
+        select(theirs[j - 1], j)
+        for k in range(1, half):
+            go(
+                remote(
+                    rows_out.at[j, k], recv.at[j, k], s2.at[j, k], r2.at[j, k], {"sp": peers[k]}
+                )
+            )
     for fetch in fetches:
         fetch.wait()
-    for i in range(len(rounds) + behind):
-        for k in rounds[i + ahead] if i + ahead < len(rounds) else ():
-            relay(k)
-        if i == 0:
-            for copy in swaps:
-                copy.wait_recv()
-        if i < len(rounds):
-            compute(rounds[i])
-        for k in rounds[i - behind] if i >= behind else ():
-            combine(k)
+    for copy in swaps:
+        copy.wait_recv()
+    for step in "r4 c0 r5 c1 c4 b0 r6 c5 b4 b1 c2 r7 c6 b5 b2 c3 c7 b6 b3 b7".split():
+        ks = eighth(int(step[1:]))
+        if step[0] == "c":
+            compute(ks)
+        else:
+            for k in ks:
+                (relay if step[0] == "r" else combine)(k)
 
     answers = []
     for k in range(n_sp):
@@ -518,7 +564,8 @@
         + [pltpu.VMEM(a.shape, a.dtype) for a in small]
         + [
             pltpu.VMEM((share, model), f32),
-            pltpu.VMEM((n_sp,) + block, bf16),
+            pltpu.VMEM((n_hi, share, model), bf16),
+            pltpu.VMEM((n_hi, n_sp) + block, bf16),
             pltpu.VMEM((n_hi, n_sp) + block, bf16),
             pltpu.VMEM((n_sp,) + block, f32),
             pltpu.VMEM((n_hi, n_sp) + block, bf16),
@@ -532,6 +579,8 @@
             dma((3,)),
             dma((3,)),
             dma((3,)),
+            dma((n_hi,)),
+            dma((n_hi,)),
             dma((n_sp,)),
             dma((n_sp,)),
             dma((n_hi, n_sp)),

time: 61.4 us -> 57.7 us (0.940)
  Pallas kernels: 59.7 us -> 56 us
    pallas_call x1, Pallas kernels: 59.7 us -> 56 us  [on_device(): pl.pallas_call(functools.partial(layer_kernel, n_sp, n_tp, slots), out_sh...]
where the time goes in v2:
time: 57.7 us; the launch traced here: 57.6 us
  Pallas kernels  56 us (97%)
  local copies, waits for them, and re-layouts  1.62 us (3%)
    pallas_call x1, Pallas kernels, on_device(): pl.pallas_call(functools.partial(layer_kernel, n_sp, n_tp, slots), out_sh...  56 us
    unnamed x1, local copies, waits for them, and re-layouts  1.62 us

profile of v2, /device:TPU:0, one launch (start us, length us, event | category | flops | bytes accessed | tf_op | source)
XLA Modules:
  0.0 57.6 jit_solution(1349258285715992310)
XLA Ops:
  0.0 56.0 %layer.1 = bf16[48,2048]{1,0:T(8,128)(2,1)} custom-call(bf16[192,128]{1,0:T(8,128)(2,1)} %refs_0_.1, f32[8,192]{1,0:T(8,128)} %bitcast.15, f32[2,8,64]{2,1,0:T(8,128)} %refs_2_.1, f32[2,8,64]{2,1,0:T(8,128)} %refs_3_.1, f32[2,128,64]{2,1,0:T(8,128)} %bitcast.11, f32[2,128,64]{2,1,0:T(8,128)} %bitcast.12, f32[2,128,64]{2,1,0:T(8,128)} %bitcast.13, ...), custom_call_target="tpu_custom_call" | custom-call | tf_op jit(solution)/shard_map/layer/pallas_call | solution.py:543
  56.0 1.6 %copy.21 = bf16[48,2048]{1,0:T(8,128)(2,1)} copy(bf16[48,2048]{1,0:T(8,128)(2,1)} %layer.1) | data formatting | bytes 393216

commit v3 on v2

--- a/solution.py
+++ b/solution.py
@@ -29,7 +29,15 @@
     return lax.dot_general(a, b, (dims, ((), ())), precision=highest, preferred_element_type=f32)
 
 
-def mixer_body(n_sp, n_tp, early, linked, sends, refs):
+def pieces(values, count):
+    out = []
+    for _ in range(count):
+        out.append(values.astype(bf16))
+        values = values - out[-1].astype(f32)
+    return out
+
+
+def mixer_body(n_sp, n_tp, early, linked, idle, sends, refs):
     sources, staged = refs[:12], refs[12:24]
     (push, gate, seg, enter, total, totals, act, chan) = refs[24:32]
     (stage_sems, send_a, recv_a, send_b, recv_b) = refs[32:]
@@ -60,20 +68,29 @@
     order = iota((length, length), 0)
     place = iota((length, length), 1)
     shuffle = (place == (order % segments) * steps + order // segments).astype(f32)
-    x = jnp.dot(shuffle.astype(bf16), x_ref[...], preferred_element_type=f32)
-    spread = (iota((states, width), 1) % states == iota((states, width), 0)).astype(f32)
+    shuffle = shuffle.astype(bf16)
+    x = jnp.dot(shuffle, x_ref[...], preferred_element_type=f32)
     own = iota((groups, width), 1) // states == iota((groups, width), 0)
     diagonal = iota((channels, width), 1) // states == iota((channels, width), 0) // each
 
+    def wide(values):
+        return jnp.concatenate([values] * groups, axis=1)
+
     def row(values):
-        wide = exact_dot(values, spread)
-        return jnp.sum(jnp.where(own, wide, 0.0), axis=0, keepdims=True)
+        return jnp.sum(jnp.where(own, wide(values), 0.0), axis=0, keepdims=True)
 
     def table(values):
-        return jnp.where(diagonal, exact_dot(values, spread), 0.0)
-
-    gates = exact_dot(shuffle, jnp.exp(gate_ref[...]), ((1,), (1,)))
-    gate[...] = exact_dot(gates, own.astype(f32))
+        return jnp.where(diagonal, wide(values), 0.0)
+
+    gates = jnp.concatenate(pieces(jnp.exp(gate_ref[...]), 3), axis=0)
+    gates = lax.dot_general(shuffle, gates, (((1,), (1,)), ((), ())), preferred_element_type=f32)
+    gate[...] = jnp.dot(
+        gates.astype(bf16),
+        jnp.concatenate([own.astype(f32).astype(bf16)] * 3, axis=0),
+        preferred_element_type=f32,
+    )
+    twice = x.astype(bf16)
+    twice = jnp.concatenate([twice, twice], axis=1)
     turn_rows = []
     for k in range(2):
         rate = decay_ref[k]
@@ -81,8 +98,9 @@
         retain = jnp.exp(-rate)
         scale = row(jnp.sqrt(1.0 - jnp.exp(-2.0 * rate)))
         turn_rows.append((row(retain * jnp.cos(turn)), row(retain * jnp.sin(turn))))
-        push[2 * k] = exact_dot(x, table(drive_re[k]) * scale)
-        push[2 * k + 1] = exact_dot(x, table(drive_im[k]) * scale)
+        for i, drive in enumerate((drive_re, drive_im)):
+            split = jnp.concatenate(pieces(table(drive[k]) * scale, 2), axis=0)
+            push[2 * k + i] = jnp.dot(twice, split, preferred_element_type=f32)
     (f_re, f_im), (b_re, b_im) = turn_rows
 
     zero = jnp.zeros((segments, width), f32)
@@ -95,20 +113,32 @@
         out = []
         for k, (sr, si) in enumerate(((f_re, f_im), (b_re, b_im))):
             at = rows_of(j if k == 0 else steps - 1 - j)
-            ar, ai, vr, vi = c[4 * k : 4 * k + 4]
+            kept, vr, vi = c[3 * k : 3 * k + 3]
             g = gate[at, :]
             mr, mi = g * sr, g * si
             out += [
-                mr * ar - mi * ai,
-                mr * ai + mi * ar,
+                kept * g,
                 mr * vr - mi * vi + push[2 * k, at, :],
                 mr * vi + mi * vr + push[2 * k + 1, at, :],
             ]
         return tuple(out)
 
-    ends = lax.fori_loop(0, steps, first, (one, zero, zero, zero) * 2)
-    for i, part in enumerate(ends):
-        seg[i] = part
+    def times(a, b):
+        return (a[0] * b[0] - a[1] * b[1], a[0] * b[1] + a[1] * b[0])
+
+    def power(base, count):
+        if count == 1:
+            return base
+        root = power(base, count // 2)
+        root = times(root, root)
+        return times(root, base) if count % 2 else root
+
+    ends = lax.fori_loop(0, steps, first, (one, zero, zero) * 2, unroll=4)
+    for k, turned in enumerate(turn_rows):
+        kept, vr, vi = ends[3 * k : 3 * k + 3]
+        full = power(turned, steps)
+        for i, part in enumerate((kept * full[0], kept * full[1], vr, vi)):
+            seg[4 * k + i] = part
 
     def link(parts, c):
         ar, ai, vr, vi = parts
@@ -157,7 +187,9 @@
     linked()
     for load in loads[6:9]:
         load.wait()
-    tables = [(table(read_re[k]), table(read_im[k])) for k in range(2)]
+    tables = [value for k in range(2) for value in (table(read_re[k]), -table(read_im[k]))]
+    tables = jnp.concatenate(pieces(jnp.concatenate(tables, axis=1), 2), axis=0)
+    direct = skip_ref[...] * x
     for k in range(1, n_sp):
         arrival(k).wait_recv()
 
@@ -186,16 +218,18 @@
             out += [new_re, new_im]
         return tuple(out)
 
-    lax.fori_loop(0, steps, second, tuple(enter[i] for i in range(4)))
-    over = ((1,), (1,))
-    readout = exact_dot(push[0], tables[0][0], over) - exact_dot(push[1], tables[0][1], over)
-    readout = readout + (
-        exact_dot(push[2], tables[1][0], over) - exact_dot(push[3], tables[1][1], over)
-    )
-    readout = readout + skip_ref[...] * x
+    lax.fori_loop(0, steps, second, tuple(enter[i] for i in range(4)), unroll=4)
+    over = (((1,), (1,)), ((), ()))
+    readout = direct
+    for i in range(4):
+        at = slice(i * width, (i + 1) * width)
+        coarse, fine = pieces(push[i], 2)
+        both = lax.dot_general(coarse, tables[:, at], over, preferred_element_type=f32)
+        rest = lax.dot_general(fine, tables[:channels, at], over, preferred_element_type=f32)
+        readout = readout + (both[:, :channels] + (both[:, channels:] + rest))
     mixed = jax.nn.gelu(readout).astype(bf16)
     act[...] = lax.dot_general(
-        shuffle.astype(bf16), mixed, (((0,), (0,)), ((), ())), preferred_element_type=f32
+        shuffle, mixed, (((0,), (0,)), ((), ())), preferred_element_type=f32
     ).astype(bf16)
 
     share = length // n_tp
@@ -213,6 +247,7 @@
     for k in range(1, n_tp):
         sends.append(shift(k, True))
         sends[-1].start()
+    idle()
     chan[tp] = act[pl.ds(pl.multiple_of(tp * share, share), share), :]
     for load in loads[9:]:
         load.wait()
@@ -292,23 +327,9 @@
         for copy in swaps:
             go(copy)
 
-    middle = mixer_body(n_sp, n_tp, early, linked, sends, mixer_in + mixer_scratch)
-    middle_ref[...] = middle
-    plain[0] = middle.astype(bf16)
-
-    def across(j):
-        return {"tp": flip(hi, j) * 2 + lo}
-
-    def crossing(j):
-        return remote(plain.at[0], plain.at[j], s0.at[j], r0.at[j], across(j))
-
-    for j in range(1, n_hi):
-        go(crossing(j))
-    for copy in stages:
-        copy.wait()
     routes_ref, group_ref, shares_ref, gain_ref = small
 
-    share, model = middle.shape
+    share, model = middle_ref.shape
     length = routes_ref.shape[1]
     main, extra, fold, piece = shape_of_block(slots, model)
     per = 16 * main + 16
@@ -316,13 +337,6 @@
     masks = [line == c for c in range(fold)]
     keep = [mask.astype(f32).astype(bf16) for mask in masks]
 
-    weights = shares_ref[...]
-    weights = group_ref[...] * weights / jnp.sum(weights, axis=0, keepdims=True)
-    table = jnp.concatenate([routes_ref[...].astype(f32), weights], axis=0)
-    def look(member):
-        pick = (iota((length, share), 0) == member * share + iota((length, share), 1)).astype(f32)
-        return exact_dot(table, pick)
-
     half = max(1, n_sp // 2)
     upper = lax.div(sp, half)
     depth = sp + upper * (n_sp - 1 - 2 * sp)
@@ -333,30 +347,49 @@
     peers = [mirrored(flip(depth, k), upper) for k in range(half)]
     peers += [mirrored(k, 1 - upper) for k in range(n_sp - half)]
     mine = [k if k < half else half + depth for k in range(n_sp)]
-    expert = jnp.full((n_sp, share), sp, jnp.int32)
-    for k in range(1, n_sp):
-        expert = jnp.where(iota((n_sp, share), 0) == k, peers[k], expert)
-    expert = expert.astype(f32)
-    before = (iota((share, share), 0) < iota((share, share), 1)).astype(bf16)
-    place = iota((per, share), 0)
-    slot = jnp.where(place < 16 * main, place, 16 * main + (place - 16 * main) // fold)
-    slot = slot.astype(f32)
-
-    def choose(facts, count):
-        first, second = facts[0:1] == expert, facts[1:2] == expert
-        uses = jnp.where(first, 1.0, 0.0) + jnp.where(second, 1.0, 0.0)
-        amounts = jnp.where(first, facts[2:3], 0.0) + jnp.where(second, facts[3:4], 0.0)
-        rank = jnp.dot(uses.astype(bf16), before, preferred_element_type=f32)
-        picks = [jnp.where(slot == rank[k : k + 1], uses[k : k + 1], 0.0) for k in range(count)]
-        return picks, amounts
-
-    chosen, amounts = choose(look(tp), n_sp)
-    theirs = [choose(look(across(j)["tp"]), half)[0] for j in range(1, n_hi)]
-    weigh = jnp.concatenate([chosen[k] * amounts[k : k + 1] for k in range(n_sp)], axis=0)
-    weigh = weigh.T
-    coarse = weigh.astype(bf16)
-    fine = (weigh - coarse.astype(f32)).astype(bf16)
-    weigh = jnp.concatenate([coarse, fine], axis=0)
+    prepared = []
+
+    def idle():
+        for copy in stages:
+            copy.wait()
+        prepared.extend(prepare())
+
+    def prepare():
+        weights = shares_ref[...]
+        weights = group_ref[...] * weights / jnp.sum(weights, axis=0, keepdims=True)
+        table = jnp.concatenate([routes_ref[...].astype(f32), weights], axis=0)
+        def look(member):
+            pick = (iota((length, share), 0) == member * share + iota((length, share), 1)).astype(f32)
+            return exact_dot(table, pick)
+
+        expert = jnp.full((n_sp, share), sp, jnp.int32)
+        for k in range(1, n_sp):
+            expert = jnp.where(iota((n_sp, share), 0) == k, peers[k], expert)
+        expert = expert.astype(f32)
+        before = (iota((share, share), 0) < iota((share, share), 1)).astype(bf16)
+        place = iota((per, share), 0)
+        slot = jnp.where(place < 16 * main, place, 16 * main + (place - 16 * main) // fold)
+        slot = slot.astype(f32)
+
+        def choose(facts, count):
+            first, second = facts[0:1] == expert, facts[1:2] == expert
+            uses = jnp.where(first, 1.0, 0.0) + jnp.where(second, 1.0, 0.0)
+            amounts = jnp.where(first, facts[2:3], 0.0) + jnp.where(second, facts[3:4], 0.0)
+            rank = jnp.dot(uses.astype(bf16), before, preferred_element_type=f32)
+            picks = [jnp.where(slot == rank[k : k + 1], uses[k : k + 1], 0.0) for k in range(count)]
+            return picks, amounts
+
+        chosen, amounts = choose(look(tp), n_sp)
+        theirs = [choose(look(across(j)["tp"]), half)[0] for j in range(1, n_hi)]
+        weigh = jnp.concatenate([chosen[k] * amounts[k : k + 1] for k in range(n_sp)], axis=0)
+        weigh = weigh.T
+        coarse = weigh.astype(bf16)
+        fine = (weigh - coarse.astype(f32)).astype(bf16)
+        weigh = jnp.concatenate([coarse, fine], axis=0)
+        return chosen, theirs, weigh
+
+    def across(j):
+        return {"tp": flip(hi, j) * 2 + lo}
 
     def pack(values, extras, store):
         for i in range(main):
@@ -382,6 +415,16 @@
 
             pack(block, block[16 * main :], store)
 
+    middle = mixer_body(n_sp, n_tp, early, linked, idle, sends, mixer_in + mixer_scratch)
+    middle_ref[...] = middle
+    plain[0] = middle.astype(bf16)
+
+    def crossing(j):
+        return remote(plain.at[0], plain.at[j], s0.at[j], r0.at[j], across(j))
+
+    for j in range(1, n_hi):
+        go(crossing(j))
+    chosen, theirs, weigh = prepared
     select(chosen, 0)
 
     def arrive(k):

time: 57.7 us -> 54.4 us (0.943)
  Pallas kernels: 56 us -> 52.6 us
    pallas_call x1, Pallas kernels: 56 us -> 52.6 us  [on_device(): pl.pallas_call(functools.partial(layer_kernel, n_sp, n_tp, slots), out_sh...]
where the time goes in v3:
time: 54.4 us; the launch traced here: 54.3 us
  Pallas kernels  52.6 us (97%)
  local copies, waits for them, and re-layouts  1.62 us (3%)
    pallas_call x1, Pallas kernels, on_device(): pl.pallas_call(functools.partial(layer_kernel, n_sp, n_tp, slots), out_sh...  52.6 us
    unnamed x1, local copies, waits for them, and re-layouts  1.62 us

profile of v3, /device:TPU:0, one launch (start us, length us, event | category | flops | bytes accessed | tf_op | source)
XLA Modules:
  0.0 54.3 jit_solution(14232069521071888830)
XLA Ops:
  0.0 52.6 %layer.1 = bf16[48,2048]{1,0:T(8,128)(2,1)} custom-call(bf16[192,128]{1,0:T(8,128)(2,1)} %refs_0_.1, f32[8,192]{1,0:T(8,128)} %bitcast.15, f32[2,8,64]{2,1,0:T(8,128)} %refs_2_.1, f32[2,8,64]{2,1,0:T(8,128)} %refs_3_.1, f32[2,128,64]{2,1,0:T(8,128)} %bitcast.11, f32[2,128,64]{2,1,0:T(8,128)} %bitcast.12, f32[2,128,64]{2,1,0:T(8,128)} %bitcast.13, ...), custom_call_target="tpu_custom_call" | custom-call | tf_op jit(solution)/shard_map/layer/pallas_call | solution.py:586
  52.6 1.6 %copy.21 = bf16[48,2048]{1,0:T(8,128)(2,1)} copy(bf16[48,2048]{1,0:T(8,128)(2,1)} %layer.1) | data formatting | bytes 393216

commit v4 on v3

--- a/solution.py
+++ b/solution.py
@@ -184,7 +184,6 @@
     for k in range(1, n_sp):
         sends.append(hand(k))
         sends[-1].start()
-    linked()
     for load in loads[6:9]:
         load.wait()
     tables = [value for k in range(2) for value in (table(read_re[k]), -table(read_im[k]))]
@@ -193,6 +192,7 @@
     for k in range(1, n_sp):
         arrival(k).wait_recv()
 
+    linked()
     for k in range(2):
         c = (zero[:1], zero[:1])
         for d in range(n_sp) if k == 0 else range(n_sp - 1, -1, -1):
@@ -345,8 +345,12 @@
         return index + side * (n_sp - 1 - 2 * index)
 
     peers = [mirrored(flip(depth, k), upper) for k in range(half)]
-    peers += [mirrored(k, 1 - upper) for k in range(n_sp - half)]
-    mine = [k if k < half else half + depth for k in range(n_sp)]
+    quarter = max(1, half // 2)
+    outer = lax.div(depth, quarter) * quarter
+    inner = depth - outer
+    rest = range(n_sp - half)
+    peers += [mirrored(k // quarter * quarter + flip(inner, k % quarter), 1 - upper) for k in rest]
+    mine = [k if k < half else half + outer + k % quarter for k in range(n_sp)]
     prepared = []
 
     def idle():
@@ -496,7 +500,7 @@
     def eighth(i):
         return range(i * unit, i * unit + unit)
 
-    for i in (0, 1, 4, 6, 5, 7, 2, 3):
+    for i in (0, 1, 5, 7, 4, 6, 2, 3):
         for k in eighth(i):
             if k:
                 there = mine[k]
@@ -522,7 +526,7 @@
         fetch.wait()
     for copy in swaps:
         copy.wait_recv()
-    for step in "r4 c0 r5 c1 c4 b0 r6 c5 b4 b1 c2 r7 c6 b5 b2 c3 c7 b6 b3 b7".split():
+    for step in "r5 c0 r4 c5 c1 b0 r7 c4 b5 b1 c2 r6 c7 b4 b2 c3 c6 b7 b3 b6".split():
         ks = eighth(int(step[1:]))
         if step[0] == "c":
             compute(ks)
@@ -585,7 +589,7 @@
     block = (16, main * model + piece)
     return pl.pallas_call(
         functools.partial(layer_kernel, n_sp, n_tp, slots),
-        out_shape=jax.ShapeDtypeStruct((share, model), bf16),
+        out_shape=pltpu.VMEM((share, model), bf16),
         in_specs=[pl.BlockSpec(memory_space=pl.ANY)] * len(operands),
         out_specs=pl.BlockSpec(memory_space=pltpu.VMEM),
         scratch_shapes=[pltpu.VMEM(a.shape, a.dtype) for a in staged]

time: 54.4 us -> 50.7 us (0.932); the launches traced: 54.3 us -> 50 us
  Pallas kernels: 52.6 us -> 49.3 us
  local copies, waits for them, and re-layouts: 1.62 us -> 0.68 us
    pallas_call x1, Pallas kernels: 52.6 us -> 49.3 us  [on_device(): pl.pallas_call(functools.partial(layer_kernel, n_sp, n_tp, slots), out_sh...]
    unnamed x1, local copies, waits for them, and re-layouts: 1.62 us -> 0.68 us
where the time goes in v4:
time: 50.7 us; the launch traced here: 50 us
  Pallas kernels  49.3 us (97%)
  local copies, waits for them, and re-layouts  0.68 us (1%)
    pallas_call x1, Pallas kernels, on_device(): pl.pallas_call(functools.partial(layer_kernel, n_sp, n_tp, slots), out_sh...  49.3 us

profile of v4, /device:TPU:0, one launch (start us, length us, event | category | flops | bytes accessed | tf_op | source)
XLA Modules:
  0.0 50.0 jit_solution(1793193599666219809)
XLA Ops:
  0.0 49.3 %layer.1 = bf16[48,2048]{1,0:T(8,128)(2,1)S(1)} custom-call(bf16[192,128]{1,0:T(8,128)(2,1)} %refs_0_.1, f32[8,192]{1,0:T(8,128)} %bitcast.15, f32[2,8,64]{2,1,0:T(8,128)} %refs_2_.1, f32[2,8,64]{2,1,0:T(8,128)} %refs_3_.1, f32[2,128,64]{2,1,0:T(8,128)} %bitcast.11, f32[2,128,64]{2,1,0:T(8,128)} %bitcast.12, f32[2,128,64]{2,1,0:T(8,128)} %bitcast.13, ...), custom_call_target="tpu_custom_call" | custom-call | tf_op jit(solution)/shard_map/layer/pallas_call | solution.py:590
  49.3 0.7 %copy.21 = bf16[48,2048]{1,0:T(8,128)(2,1)} copy(bf16[48,2048]{1,0:T(8,128)(2,1)S(1)} %layer.1) | data formatting | bytes 393216

commit v5 on v4

--- a/solution.py
+++ b/solution.py
@@ -526,7 +526,7 @@
         fetch.wait()
     for copy in swaps:
         copy.wait_recv()
-    for step in "r5 c0 r4 c5 c1 b0 r7 c4 b5 b1 c2 r6 c7 b4 b2 c3 c6 b7 b3 b6".split():
+    for step in "r5 c0 r4 c5 c1 b0 r7 c4 b5 c2 b1 r6 c7 b4 c3 b2 c6 b7 b3 b6".split():
         ks = eighth(int(step[1:]))
         if step[0] == "c":
             compute(ks)

time: 50.7 us -> 50.3 us (level)
  the two profiles are of different devices: /device:TPU:0 before, /device:TPU:17 now
where the time goes in v5:
time: 50.3 us; the launch traced here: 50.2 us
  Pallas kernels  49.5 us (98%)
  local copies, waits for them, and re-layouts  0.68 us (1%)
    pallas_call x1, Pallas kernels, on_device(): pl.pallas_call(functools.partial(layer_kernel, n_sp, n_tp, slots), out_sh...  49.5 us

profile of v5, /device:TPU:17, one launch (start us, length us, event | category | flops | bytes accessed | tf_op | source)
XLA Modules:
  0.0 50.2 jit_solution(9424288524691280156)
XLA Ops:
  0.0 49.5 %layer.1 = bf16[48,2048]{1,0:T(8,128)(2,1)S(1)} custom-call(bf16[192,128]{1,0:T(8,128)(2,1)} %refs_0_.1, f32[8,192]{1,0:T(8,128)} %bitcast.15, f32[2,8,64]{2,1,0:T(8,128)} %refs_2_.1, f32[2,8,64]{2,1,0:T(8,128)} %refs_3_.1, f32[2,128,64]{2,1,0:T(8,128)} %bitcast.11, f32[2,128,64]{2,1,0:T(8,128)} %bitcast.12, f32[2,128,64]{2,1,0:T(8,128)} %bitcast.13, ...), custom_call_target="tpu_custom_call" | custom-call | tf_op jit(solution)/shard_map/layer/pallas_call | solution.py:590
  49.5 0.7 %copy.21 = bf16[48,2048]{1,0:T(8,128)(2,1)} copy(bf16[48,2048]{1,0:T(8,128)(2,1)S(1)} %layer.1) | data formatting | bytes 393216
